TPU v7x, 512 devices: a whole 4x8x8 slice. The times are simulated.
512 devices in a mesh: sp: 32 (over z, x), tp: 16 (over y, core).
Axes of the slice: x: 4, y: 8, z: 8, core: 2. Of those that a mesh axis runs over, the one named last changes fastest.
Arguments:
- stream: bfloat16 [4096, 2048], P('sp'), may hold values from -15 to 15
- cotangent: bfloat16 [4096, 2048], P('sp'), may hold values from -6 to 6
- route_ids: int32 [4096, 2], P('sp'), may hold values from 0 to 31, all different within a row; in each aligned block of 128 rows (0 to 127, 128 to 255, ...) at most 16 rows name the same one
- route_weights: float32 [4096, 2], P('sp'), may hold values from 0.1 to 0.9
- w_gate: bfloat16 [32, 2048, 2048], P('sp', None, 'tp'), may hold values from -0.125 to 0.125
- w_up: bfloat16 [32, 2048, 2048], P('sp', None, 'tp'), may hold values from -0.125 to 0.125
- w_down: bfloat16 [32, 2048, 2048], P('sp', 'tp'), may hold values from -0.125 to 0.125
- out_proj: bfloat16 [2048, 512], P(None, 'tp'), may hold values from -0.25 to 0.25
- mixed: bfloat16 [512, 4096], P('tp', 'sp'), may hold values from -6 to 6
- rec_input: bfloat16 [512, 4096], P('tp', 'sp'), may hold values from -6 to 6
- branch_input: bfloat16 [512, 4096], P('tp', 'sp'), may hold values from -6 to 6
- state_before: float32 [512, 4096], P('tp', 'sp'), may hold values from -6 to 6
- rec_gates: bfloat16 [16, 32, 32], P('tp'), may hold values from -1 to 1
- in_gates: bfloat16 [16, 32, 32], P('tp'), may hold values from -1 to 1
- decay_param: float32 [512], P('tp'), may hold values from 4.4 to 11
- decay_shift: float32 [512, 4096], P('tp', 'sp'), may hold values from -1.4 to -1e-05
Outputs:
- grad_gate: bfloat16 [32, 2048, 2048], P('sp', None, 'tp')
- grad_up: bfloat16 [32, 2048, 2048], P('sp', None, 'tp')
- grad_down: bfloat16 [32, 2048, 2048], P('sp', 'tp')
- grad_proj: float32 [2048, 512], P('sp', 'tp')
- grad_rec: float32 [512, 4096], P('tp', 'sp')
- grad_branch: float32 [512, 4096], P('tp', 'sp')
Inputs may be any that keep to these rules, and one draw needn't show every extreme that they name: `route_ids`: each row names 2 different experts; the rows of one device name no expert more than 16 times, a bound that some block reaches on some device.
All inputs are finite; a program needn't handle non-finite values.
Results may differ from a plain program's by a relative error of at most 0.03.
Values may be sent and summed in bfloat16 or wider, within the bound.
No kernel may reach another device: no remote copies, remote signals or barrier semaphores. Data moves between devices by JAX's collectives and lax.ppermute only.
A program may use at most 64 MiB of HBM per device.

v0:
```python
import jax
import jax.numpy as jnp
from jax import lax
from jax.sharding import PartitionSpec as P

RATE_SCALE = 8.0
CLAMP_LIMIT = 7.0
GLU_ALPHA = 1.702


def in_one_piece(arrays, axis, split_dim, concat_dim, along):
    widths = [a.shape[along] for a in arrays]
    both = jnp.concatenate(arrays, axis=along)
    filled = lax.all_to_all(both, axis, split_axis=split_dim, concat_axis=concat_dim, tiled=True)
    return tuple(jnp.split(filled, [sum(widths[:k]) for k in range(1, len(widths))], axis=along))


def split_up(array, dim, size):
    before, after = (array.shape[:dim], array.shape[dim + 1 :])
    return jnp.moveaxis(array.reshape(*before, size, -1, *after), dim, 0)


def sum_at_owner(array, axis, dim):
    size = lax.axis_size(axis)
    tiles = lax.all_to_all(split_up(array, dim, size), axis, 0, 0, tiled=True)
    return jnp.sum(tiles.astype(jnp.float32), axis=0)


def sent_to_all(array, axis):
    size = lax.axis_size(axis)
    return lax.all_to_all(
        jnp.broadcast_to(array[None], (size, *array.shape)), axis, 0, 0, tiled=True
    )


def all_in_one(array, axis):
    leaves = jax.tree.leaves(array)
    order = sorted(range(len(leaves)), key=lambda k: -leaves[k].size)
    width = (1, *leaves[order[0]].shape)[-1]
    lines = [
        jnp.pad(leaves[k].reshape(-1), (0, -leaves[k].size % width)).reshape(-1, width)
        for k in order
    ]
    both, at, found = (sent_to_all(jnp.concatenate(lines), axis), 0, {})
    for k, line in zip(order, lines):
        slab = both[:, at : at + len(line)].reshape(len(both), -1)
        found[k] = slab[:, : leaves[k].size].reshape(-1, *leaves[k].shape)
        at += len(line)
    numbers = iter(range(len(leaves)))
    return jax.tree.map(lambda _: found[next(numbers)], array)


def folded_in_pairs(pieces, combine):
    while len(jax.tree.leaves(pieces)[0]) > 1:
        pieces = jax.vmap(combine)(
            *(jax.tree.map(lambda part: part[side::2], pieces) for side in (0, 1))
        )
    return jax.tree.map(lambda part: part[0], pieces)


def carried_in(array, axis, combine, identity):
    size, position = (lax.axis_size(axis), lax.axis_index(axis))
    passed = jnp.arange(size) > position

    def kept(part, zero, own):
        part = jnp.where(
            passed.reshape(-1, *(1 for _ in own.shape)), part, jnp.asarray(zero, own.dtype)
        )
        return part[::-1]

    pieces = all_in_one(array, axis)
    return folded_in_pairs(jax.tree.map(kept, pieces, identity, array), combine)


def expert_act(gate_pre, up_pre):
    glu_part = jnp.minimum(gate_pre, CLAMP_LIMIT)
    lin_part = jnp.clip(up_pre, -CLAMP_LIMIT, CLAMP_LIMIT)
    return glu_part * jax.nn.sigmoid(GLU_ALPHA * glu_part) * (lin_part + 1.0)


def reverse_step(later_elem, earlier_elem):
    return (later_elem[0] * earlier_elem[0], earlier_elem[1] + earlier_elem[0] * later_elem[1])


def compose_maps(higher_map, lower_map):
    return (lower_map[0] * higher_map[0], lower_map[0] * higher_map[1] + lower_map[1])


def weight_grads(tokens_in, grads_in, d_gate, d_up, act_low):
    g_gate = jnp.einsum("secd,secf->edf", tokens_in, d_gate, preferred_element_type=jnp.float32)
    g_up = jnp.einsum("secd,secf->edf", tokens_in, d_up, preferred_element_type=jnp.float32)
    g_down = jnp.einsum("secf,secd->efd", act_low, grads_in, preferred_element_type=jnp.float32)
    return (g_gate.astype(jnp.bfloat16), g_up.astype(jnp.bfloat16), g_down.astype(jnp.bfloat16))


def local(
    stream,
    cotangent,
    route_ids,
    route_weights,
    w_gate,
    w_up,
    w_down,
    out_proj,
    mixed,
    rec_input,
    branch_input,
    state_before,
    rec_gates,
    in_gates,
    decay_param,
    decay_shift,
):
    sp_count = lax.axis_size("sp")
    tok_rows, model_width = cotangent.shape
    top_count = route_ids.shape[1]
    local_experts = w_gate.shape[0]
    expert_count = local_experts * sp_count
    capacity = 2 * tok_rows * top_count // expert_count
    flat_ids = route_ids.reshape(-1)
    onehot = (flat_ids[:, None] == jnp.arange(expert_count, dtype=jnp.int32)[None, :]).astype(
        jnp.int32
    )
    slot_index = jnp.sum((jnp.cumsum(onehot, axis=0) - onehot) * onehot, axis=1)
    target = flat_ids * capacity + slot_index
    scaled = (route_weights[:, :, None] * cotangent[:, None, :].astype(jnp.float32)).astype(
        jnp.bfloat16
    )
    scaled = scaled.reshape(-1, model_width)
    copies = jnp.broadcast_to(stream[:, None, :], (tok_rows, top_count, model_width)).reshape(
        -1, model_width
    )
    empty_rows = jnp.zeros((expert_count * capacity, model_width), jnp.bfloat16)
    rows_sent = empty_rows.at[target].set(scaled)
    tokens_sent = empty_rows.at[target].set(copies)
    grads_in, tokens_in = in_one_piece((rows_sent, tokens_sent), "sp", 0, 0, 1)
    grads_in = grads_in.reshape(sp_count, local_experts, capacity, model_width)
    tokens_in = tokens_in.reshape(sp_count, local_experts, capacity, model_width)
    gate_pre = jnp.einsum("secd,edf->secf", tokens_in, w_gate, preferred_element_type=jnp.float32)
    up_pre = jnp.einsum("secd,edf->secf", tokens_in, w_up, preferred_element_type=jnp.float32)
    act_val, act_vjp = jax.vjp(expert_act, gate_pre, up_pre)
    act_low = act_val.astype(jnp.bfloat16)
    d_act = jnp.einsum("secd,efd->secf", grads_in, w_down, preferred_element_type=jnp.float32)
    d_gate, d_up = act_vjp(d_act)
    d_gate = d_gate.astype(jnp.bfloat16)
    d_up = d_up.astype(jnp.bfloat16)
    grad_gate, grad_up, grad_down = weight_grads(tokens_in, grads_in, d_gate, d_up, act_low)
    partial_value = jnp.einsum("secf,edf->secd", d_gate, w_gate, preferred_element_type=jnp.float32)
    partial_value = partial_value + jnp.einsum(
        "secf,edf->secd", d_up, w_up, preferred_element_type=jnp.float32
    )
    share = sum_at_owner(partial_value.astype(jnp.bfloat16), "tp", 3).astype(jnp.bfloat16)
    share_cols = share.shape[3]
    returned = lax.all_to_all(
        share.reshape(-1, share_cols), "sp", split_axis=0, concat_axis=0, tiled=True
    )
    per_pair = returned[target].astype(jnp.float32).reshape(tok_rows, top_count, share_cols)
    own_cols = lax.dynamic_slice_in_dim(cotangent, lax.axis_index("tp") * share_cols, share_cols, 1)
    share_low = (own_cols.astype(jnp.float32) + jnp.sum(per_pair, axis=1)).astype(jnp.bfloat16)
    stream_low = lax.all_gather(share_low, "tp", axis=1, tiled=True)
    d_mixed = lax.dot_general(
        out_proj, stream_low, (((0,), (1,)), ((), ())), preferred_element_type=jnp.float32
    )
    grad_proj = sum_at_owner(
        lax.dot_general(
            stream_low, mixed, (((0,), (1,)), ((), ())), preferred_element_type=jnp.float32
        ).astype(jnp.bfloat16),
        "sp",
        0,
    )
    channels, positions = rec_input.shape
    gate_heads = rec_gates.shape[0]
    head_dim = rec_gates.shape[1]
    rec_heads = rec_input.reshape(gate_heads, head_dim, positions)
    rec_pre = jnp.einsum(
        "hij,hit->hjt", rec_gates, rec_heads, preferred_element_type=jnp.float32
    ).reshape(channels, positions)
    in_pre = jnp.einsum(
        "hij,hit->hjt", in_gates, rec_heads, preferred_element_type=jnp.float32
    ).reshape(channels, positions)
    rec_gate = jax.nn.sigmoid(rec_pre)
    in_gate = jax.nn.sigmoid(in_pre)
    soft_plus = jax.nn.softplus(-decay_param)[:, None]
    log_decay = -RATE_SCALE * rec_gate * soft_plus + decay_shift
    decay_rate = jnp.exp(log_decay)
    token_position = lax.axis_index("sp") * positions + jnp.arange(positions, dtype=jnp.int32)
    at_start = (token_position == 0)[None, :]
    raw_mult = jnp.sqrt(-jnp.expm1(2.0 * log_decay))
    multiplier = jnp.where(at_start, 1.0, raw_mult)
    rec_value = rec_input.astype(jnp.float32)
    state_now = decay_rate * state_before + multiplier * in_gate * rec_value
    gelu_val, gelu_vjp = jax.vjp(jax.nn.gelu, branch_input.astype(jnp.float32))
    grad_branch = gelu_vjp(d_mixed * state_now)[0]
    d_state = d_mixed * gelu_val
    next_decay = jnp.concatenate([decay_rate[:, 1:], jnp.zeros((channels, 1), jnp.float32)], axis=1)
    local_adj = lax.associative_scan(reverse_step, (next_decay, d_state), reverse=True, axis=1)[1]
    log_cumsum = jnp.cumsum(log_decay, axis=1)
    total_log = log_cumsum[:, -1:]
    tail_decay = jnp.exp(total_log - log_cumsum)
    device_prod = jnp.exp(total_log[:, 0])
    head_term = decay_rate[:, 0] * local_adj[:, 0]
    identity = (jnp.ones((channels,), jnp.float32), jnp.zeros((channels,), jnp.float32))
    carried = carried_in((device_prod, head_term), "sp", compose_maps, identity)
    adjoint = local_adj + tail_decay * carried[1][:, None]
    mult_term = adjoint * in_gate * rec_value * decay_rate * decay_rate / raw_mult
    d_log = adjoint * state_before * decay_rate - jnp.where(at_start, 0.0, mult_term)
    d_rec_pre = (d_log * -RATE_SCALE * soft_plus * rec_gate * (1.0 - rec_gate)).astype(jnp.bfloat16)
    d_in_pre = (adjoint * multiplier * rec_value * in_gate * (1.0 - in_gate)).astype(jnp.bfloat16)
    back_rec = jnp.einsum(
        "hij,hjt->hit",
        rec_gates,
        d_rec_pre.reshape(gate_heads, head_dim, positions),
        preferred_element_type=jnp.float32,
    )
    back_in = jnp.einsum(
        "hij,hjt->hit",
        in_gates,
        d_in_pre.reshape(gate_heads, head_dim, positions),
        preferred_element_type=jnp.float32,
    )
    grad_rec = adjoint * multiplier * in_gate + (back_rec + back_in).reshape(channels, positions)
    return (grad_gate, grad_up, grad_down, grad_proj, grad_rec, grad_branch)


def solution(mesh):
    placed = (
        P("sp", None),
        P("sp", None),
        P("sp", None),
        P("sp", None),
        P("sp", None, "tp"),
        P("sp", None, "tp"),
        P("sp", "tp", None),
        P(None, "tp"),
        P("tp", "sp"),
        P("tp", "sp"),
        P("tp", "sp"),
        P("tp", "sp"),
        P("tp", None, None),
        P("tp", None, None),
        P("tp"),
        P("tp", "sp"),
    )
    return jax.shard_map(
        local,
        mesh=mesh,
        in_specs=placed,
        out_specs=(
            P("sp", None, "tp"),
            P("sp", None, "tp"),
            P("sp", "tp", None),
            P("sp", "tp"),
            P("tp", "sp"),
            P("tp", "sp"),
        ),
        check_vma=False,
    )
```

profile of v0, /device:TPU:8, one launch (start us, length us, event | category | flops | bytes accessed | tf_op | source)
XLA Modules:
  0.0 272.2 jit_solution(11788468494152365258)
XLA Ops:
  0.7 0.8 broadcast_multiply_fusion
  1.4 0.8 copy.57
  3.6 1.7 broadcast_in_dim.63
  5.3 1.2 reshape.294
  6.5 2.4 mul.322
  8.9 2.7 mul.323
  12.0 4.4 %scatter_custom_fusion.1 = bf16[512,2048]{1,0:T(8,128)(2,1)} fusion(s32[256]{0:T(256)S(1)} %bitcast.230, bf16[256,2048]{1,0:T(8,128)(2,1)} %reshape.294, bf16[]{:T(256)} %constant.21.clone.1), kind=kCustom, calls=%fused_computation.33 | custom fusion | bytes 2097664 | tf_op jit(solution)/shard_map/scatter | solution.py:135
  16.4 3.8 %scatter_custom_fusion = bf16[512,2048]{1,0:T(8,128)(2,1)} fusion(s32[256]{0:T(256)S(1)} %bitcast.231, f32[256,2048]{1,0:T(8,128)S(1)} %mul.323, f32[256]{0:T(256)S(1)} %mul.320, bf16[]{:T(256)} %constant.21.clone.1), kind=kCustom, calls=%fused_computation.31 | custom fusion | flops 1048576 | bytes 4195330 | tf_op jit(solution)/shard_map/scatter | solution.py:134
  20.2 2.7 pad_maximum_fusion
  22.9 108.4 %all_to_all.36 = bf16[32,16,4096]{2,1,0:T(8,128)(2,1)S(1)} all-to-all(bf16[32,16,4096]{2,1,0:T(8,128)(2,1)S(1)} %bitcast.217), channel_id=1, replica_groups=mesh['sp'=32,'tp'=16] {'sp'}, dimensions={0} | all-to-all | bytes 8388608 | tf_op jit(solution)/shard_map/all_to_all | solution.py:14
  132.3 0.7 fusion.25
  134.1 0.8 fusion.33
  135.7 0.7 fusion.6
  136.4 1.9 copy.70
  138.3 7.7 %all-to-all-start.1 = ((bf16[16,32,1,16,128]{4,3,1,2,0:T(8,128)(2,1)}), bf16[16,32,1,16,128]{4,3,1,2,0:T(8,128)(2,1)}, u32[]{:S(2)}, u32[]{:S(2)}) async-start(bf16[16,32,1,16,128]{4,3,1,2,0:T(8,128)(2,1)} %bitcast.218), calls=%async_computation.1 | async-start | bytes 4194304 | tf_op jit(solution)/shard_map/all_to_all | solution.py:25
  146.5 1.6 fusion.4
  148.0 45.3 %all-to-all-done.1 = bf16[16,32,1,16,128]{4,3,1,2,0:T(8,128)(2,1)} async-done(((bf16[16,32,1,16,128]{4,3,1,2,0:T(8,128)(2,1)}), bf16[16,32,1,16,128]{4,3,1,2,0:T(8,128)(2,1)}, u32[]{:S(2)}, u32[]{:S(2)}) %all-to-all-start.1) | async-done | bytes 2097184 | tf_op jit(solution)/shard_map/all_to_all | solution.py:25
  193.3 2.6 reduce_sum.43
  195.9 5.6 %all-to-all-start.2 = ((bf16[32,16,128]{2,1,0:T(8,128)(2,1)}), bf16[32,16,128]{2,1,0:T(8,128)(2,1)S(1)}, u32[]{:S(2)}, u32[]{:S(2)}) async-start(bf16[32,16,128]{2,1,0:T(8,128)(2,1)} %reduce_sum.43), calls=%async_computation.2 | async-start | bytes 262144 | tf_op jit(solution)/shard_map/all_to_all | solution.py:154
  201.5 1.6 fusion.3
  203.1 1.3 fusion.5
  204.4 8.0 %all-to-all-done.2 = bf16[32,16,128]{2,1,0:T(8,128)(2,1)S(1)} async-done(((bf16[32,16,128]{2,1,0:T(8,128)(2,1)}), bf16[32,16,128]{2,1,0:T(8,128)(2,1)S(1)}, u32[]{:S(2)}, u32[]{:S(2)}) %all-to-all-start.2) | async-done | bytes 131104 | tf_op jit(solution)/shard_map/all_to_all | solution.py:154
  212.4 0.9 gather_fusion
  213.5 0.8 add_convert_fusion.1
  214.3 17.8 %all_gather.3 = bf16[128,2048]{1,0:T(8,128)(2,1)S(1)} all-gather(bf16[128,128]{1,0:T(8,128)(2,1)S(1)} %add_convert_fusion.1), channel_id=1, replica_groups=mesh['sp'=32,'tp'=16] {'tp'}, dimensions={1}, use_global_device_ids=true | all-gather | bytes 557056 | tf_op jit(solution)/shard_map/all_gather | solution.py:160
  232.1 0.9 fusion.54
  243.2 3.8 %all-to-all-start.4 = ((f32[32,2,32]{2,1,0:T(2,128)}), f32[32,2,32]{2,1,0:T(2,128)S(1)}, u32[]{:S(2)}, u32[]{:S(2)}) async-start(f32[32,2,32]{2,1,0:T(2,128)} %broadcast_in_dim.65), calls=%async_computation.4 | async-start | bytes 65536 | tf_op jit(solution)/shard_map/all_to_all | solution.py:31
  247.6 0.8 reshape.312
  248.5 8.3 %all-to-all-done.4 = f32[32,2,32]{2,1,0:T(2,128)S(1)} async-done(((f32[32,2,32]{2,1,0:T(2,128)}), f32[32,2,32]{2,1,0:T(2,128)S(1)}, u32[]{:S(2)}, u32[]{:S(2)}) %all-to-all-start.4) | async-done | bytes 8224 | tf_op jit(solution)/shard_map/all_to_all | solution.py:31
  256.8 3.9 %all-to-all-start.3 = ((bf16[32,2,1024]{2,1,0:T(2,128)(2,1)}), bf16[32,2,1024]{2,1,0:T(2,128)(2,1)S(1)}, u32[]{:S(2)}, u32[]{:S(2)}) async-start(bf16[32,2,1024]{2,1,0:T(2,128)(2,1)} %reshape.312), calls=%async_computation.3 | async-start | bytes 262144 | tf_op jit(solution)/shard_map/all_to_all | solution.py:25
  261.4 0.8 fusion.8
  262.2 9.0 %all-to-all-done.3 = bf16[32,2,1024]{2,1,0:T(2,128)(2,1)S(1)} async-done(((bf16[32,2,1024]{2,1,0:T(2,128)(2,1)}), bf16[32,2,1024]{2,1,0:T(2,128)(2,1)S(1)}, u32[]{:S(2)}, u32[]{:S(2)}) %all-to-all-start.3) | async-done | bytes 131104 | tf_op jit(solution)/shard_map/all_to_all | solution.py:25
  (176 shorter events, 17.2 us)
Async XLA Ops:
  0.6 132.4 %copy-start = (bf16[1,2048,128]{2,1,0:T(8,128)(2,1)S(1)}, bf16[1,2048,128]{2,1,0:T(8,128)(2,1)}, u32[]{:S(2)}) copy-start(bf16[1,2048,128]{2,1,0:T(8,128)(2,1)} %param.20) | copy-start | bytes 1572868
  0.6 5.9 %copy-start.4 = (bf16[128,2048]{1,0:T(8,128)(2,1)S(1)}, bf16[128,2048]{1,0:T(8,128)(2,1)}, u32[]{:S(2)}) copy-start(bf16[128,2048]{1,0:T(8,128)(2,1)} %param.17) | copy-start | bytes 1572868
  8.9 2.7 copy-start.11
  131.3 1.0 copy-start.3
  131.7 2.1 copy-start.1
  133.1 1.0 copy-start.12
  138.3 7.8 %copy-start.15 = (f32[32]{0:T(128)S(1)}, f32[32]{0:T(128)}, u32[]{:S(2)}) copy-start(f32[32]{0:T(128)} %param.30) | copy-start | bytes 388
  138.3 7.8 %copy-start.9 = (bf16[32,128]{1,0:T(8,128)(2,1)S(1)}, bf16[32,128]{1,0:T(8,128)(2,1)}, u32[]{:S(2)}) copy-start(bf16[32,128]{1,0:T(8,128)(2,1)} %param.25) | copy-start | bytes 24580
  138.3 7.8 %copy-start.13 = (bf16[1,32,32]{2,1,0:T(8,128)(2,1)S(1)}, bf16[1,32,32]{2,1,0:T(8,128)(2,1)}, u32[]{:S(2)}) copy-start(bf16[1,32,32]{2,1,0:T(8,128)(2,1)} %param.28) | copy-start | bytes 6148
  138.3 8.0 %copy-start.14 = (bf16[1,32,32]{2,1,0:T(8,128)(2,1)S(1)}, bf16[1,32,32]{2,1,0:T(8,128)(2,1)}, u32[]{:S(2)}) copy-start(bf16[1,32,32]{2,1,0:T(8,128)(2,1)} %param.29) | copy-start | bytes 6148
  138.3 55.0 %all-to-all-start.1 = ((bf16[16,32,1,16,128]{4,3,1,2,0:T(8,128)(2,1)}), bf16[16,32,1,16,128]{4,3,1,2,0:T(8,128)(2,1)}, u32[]{:S(2)}, u32[]{:S(2)}) async-start(bf16[16,32,1,16,128]{4,3,1,2,0:T(8,128)(2,1)} %bitcast.218), calls=%async_computation.1 | async-start | bytes 4194304 | tf_op jit(solution)/shard_map/all_to_all | solution.py:25
  195.9 16.6 %all-to-all-start.2 = ((bf16[32,16,128]{2,1,0:T(8,128)(2,1)}), bf16[32,16,128]{2,1,0:T(8,128)(2,1)S(1)}, u32[]{:S(2)}, u32[]{:S(2)}) async-start(bf16[32,16,128]{2,1,0:T(8,128)(2,1)} %reduce_sum.43), calls=%async_computation.2 | async-start | bytes 262144 | tf_op jit(solution)/shard_map/all_to_all | solution.py:154
  201.5 1.6 copy-start.2
  203.1 29.0 %copy-start.5 = (bf16[2048,32]{0,1:T(8,128)(2,1)S(1)}, bf16[2048,32]{0,1:T(8,128)(2,1)}, u32[]{:S(2)}) copy-start(bf16[2048,32]{0,1:T(8,128)(2,1)} %param.23) | copy-start | bytes 393220
  203.1 29.0 %copy-start.6 = (f32[32,128]{1,0:T(8,128)S(1)}, f32[32,128]{1,0:T(8,128)}, u32[]{:S(2)}) copy-start(f32[32,128]{1,0:T(8,128)} %param.31) | copy-start | bytes 49156
  203.1 29.0 %copy-start.7 = (f32[32,128]{1,0:T(8,128)S(1)}, f32[32,128]{1,0:T(8,128)}, u32[]{:S(2)}) copy-start(f32[32,128]{1,0:T(8,128)} %param.27) | copy-start | bytes 49156
  203.1 29.0 %copy-start.8 = (bf16[32,128]{1,0:T(8,128)(2,1)S(1)}, bf16[32,128]{1,0:T(8,128)(2,1)}, u32[]{:S(2)}) copy-start(bf16[32,128]{1,0:T(8,128)(2,1)} %param.26) | copy-start | bytes 24580
  233.0 14.1 %copy-start.10 = (bf16[32,128]{1,0:T(8,128)(2,1)S(1)}, bf16[32,128]{1,0:T(8,128)(2,1)}, u32[]{:S(2)}) copy-start(bf16[32,128]{1,0:T(8,128)(2,1)} %param.24) | copy-start | bytes 24580
  243.2 13.6 %all-to-all-start.4 = ((f32[32,2,32]{2,1,0:T(2,128)}), f32[32,2,32]{2,1,0:T(2,128)S(1)}, u32[]{:S(2)}, u32[]{:S(2)}) async-start(f32[32,2,32]{2,1,0:T(2,128)} %broadcast_in_dim.65), calls=%async_computation.4 | async-start | bytes 65536 | tf_op jit(solution)/shard_map/all_to_all | solution.py:31
  256.8 14.4 %all-to-all-start.3 = ((bf16[32,2,1024]{2,1,0:T(2,128)(2,1)}), bf16[32,2,1024]{2,1,0:T(2,128)(2,1)S(1)}, u32[]{:S(2)}, u32[]{:S(2)}) async-start(bf16[32,2,1024]{2,1,0:T(2,128)(2,1)} %reshape.312), calls=%async_computation.3 | async-start | bytes 262144 | tf_op jit(solution)/shard_map/all_to_all | solution.py:25
where the time goes:
time: 273 us; the launch traced here: 272 us
  blocking collectives  126 us (46%)
  waiting for transfers between devices  70.6 us (26%)
  local copies, waits for them, and re-layouts  28.7 us (11%)
  starting transfers between devices  20.9 us (8%)
  other arithmetic  13.6 us (5%)
  matrix products  10.7 us (4%)
    all_to_all x1, blocking collectives, in_one_piece(): lax.all_to_all(both, axis, split_axis=split_dim, concat_axis=concat_dim,...  108 us
    all_to_all x2, waiting for transfers between devices, sum_at_owner(): tiles = lax.all_to_all(split_up(array, dim, size), axis, 0, 0, tiled=True)  54.3 us
    all_gather x1, blocking collectives, local(): stream_low = lax.all_gather(share_low, 'tp', axis=1, tiled=True)  17.8 us
    all_to_all x2, starting transfers between devices, sum_at_owner(): tiles = lax.all_to_all(split_up(array, dim, size), axis, 0, 0, tiled=True)  11.6 us
    all_to_all x1, waiting for transfers between devices, sent_to_all(): lax.all_to_all(jnp.broadcast_to(array[None], (size, *array.shape)), axis,...  8.3 us
    all_to_all x1, waiting for transfers between devices, local(): lax.all_to_all(share.reshape(-1, share_cols), 'sp', split_axis=0, concat_...  8.05 us
    slice x41, local copies, waits for them, and re-layouts, local(): lax.associative_scan(reverse_step, (next_decay, d_state), reverse=True, a...  5.9 us
    all_to_all x1, starting transfers between devices, local(): lax.all_to_all(share.reshape(-1, share_cols), 'sp', split_axis=0, concat_...  5.58 us
  transfers between devices with their start and end apart: 4, of which 4 were waited for; matrix products, arithmetic and copies ran while one was open for 3% of the time, Pallas kernels for 0%

commit v1 on v0

--- a/solution.py
+++ b/solution.py
@@ -157,7 +157,8 @@
     per_pair = returned[target].astype(jnp.float32).reshape(tok_rows, top_count, share_cols)
     own_cols = lax.dynamic_slice_in_dim(cotangent, lax.axis_index("tp") * share_cols, share_cols, 1)
     share_low = (own_cols.astype(jnp.float32) + jnp.sum(per_pair, axis=1)).astype(jnp.bfloat16)
-    stream_low = lax.all_gather(share_low, "tp", axis=1, tiled=True)
+    copies_2 = jnp.concatenate([share_low] * lax.axis_size("tp"), axis=1)
+    stream_low = lax.all_to_all(copies_2, "tp", 1, 1, tiled=True)
     d_mixed = lax.dot_general(
         out_proj, stream_low, (((0,), (1,)), ((), ())), preferred_element_type=jnp.float32
     )

time: 273 us -> 291 us (1.066)
  the two profiles are of different devices: /device:TPU:8 before, /device:TPU:1 now
where the time goes in v1:
time: 291 us; the launch traced here: 290 us
  blocking collectives  107 us (37%)
  waiting for transfers between devices  81.9 us (28%)
  local copies, waits for them, and re-layouts  40.7 us (14%)
  starting transfers between devices  29.4 us (10%)
  other arithmetic  16.5 us (6%)
  matrix products  12.9 us (4%)
    all_to_all x1, blocking collectives, in_one_piece(): lax.all_to_all(both, axis, split_axis=split_dim, concat_axis=concat_dim,...  107 us
    all_to_all x2, waiting for transfers between devices, sum_at_owner(): tiles = lax.all_to_all(split_up(array, dim, size), axis, 0, 0, tiled=True)  54.8 us
    all_to_all x1, waiting for transfers between devices, local(): stream_low = lax.all_to_all(copies_2, 'tp', 1, 1, tiled=True)  14 us
    all_to_all x2, starting transfers between devices, sum_at_owner(): tiles = lax.all_to_all(split_up(array, dim, size), axis, 0, 0, tiled=True)  13.9 us
    unnamed x62, local copies, waits for them, and re-layouts  11.6 us
    all_to_all x1, waiting for transfers between devices, sent_to_all(): lax.all_to_all(jnp.broadcast_to(array[None], (size, *array.shape)), axis,...  7.08 us
    all_to_all x1, starting transfers between devices, local(): stream_low = lax.all_to_all(copies_2, 'tp', 1, 1, tiled=True)  6.43 us
    all_to_all x1, waiting for transfers between devices, local(): lax.all_to_all(share.reshape(-1, share_cols), 'sp', split_axis=0, concat_...  6.01 us
  transfers between devices with their start and end apart: 5, of which 5 were waited for; matrix products, arithmetic and copies ran while one was open for 4% of the time, Pallas kernels for 0%

profile of v1, /device:TPU:1, one launch (start us, length us, event | category | flops | bytes accessed | tf_op | source)
XLA Modules:
  0.0 289.9 jit_solution(8327993831874759691)
XLA Ops:
  3.6 1.7 broadcast_in_dim.63
  5.3 1.2 reshape.296
  6.5 2.4 mul.322
  8.9 2.7 mul.323
  12.0 4.4 %scatter_custom_fusion.1 = bf16[512,2048]{1,0:T(8,128)(2,1)} fusion(s32[256]{0:T(256)S(1)} %bitcast.235, bf16[256,2048]{1,0:T(8,128)(2,1)} %reshape.296, bf16[]{:T(256)} %constant.21.clone.1), kind=kCustom, calls=%fused_computation.33 | custom fusion | bytes 2097664 | tf_op jit(solution)/shard_map/scatter | solution.py:135
  16.4 3.8 %scatter_custom_fusion = bf16[512,2048]{1,0:T(8,128)(2,1)} fusion(s32[256]{0:T(256)S(1)} %bitcast.236, f32[256,2048]{1,0:T(8,128)S(1)} %mul.323, f32[256]{0:T(256)S(1)} %mul.320, bf16[]{:T(256)} %constant.21.clone.1), kind=kCustom, calls=%fused_computation.31 | custom fusion | flops 1048576 | bytes 4195330 | tf_op jit(solution)/shard_map/scatter | solution.py:134
  20.2 2.7 pad_maximum_fusion
  22.9 107.1 %all_to_all.48 = bf16[32,16,4096]{2,1,0:T(8,128)(2,1)S(1)} all-to-all(bf16[32,16,4096]{2,1,0:T(8,128)(2,1)S(1)} %bitcast.219), channel_id=1, replica_groups=mesh['sp'=32,'tp'=16] {'sp'}, dimensions={0} | all-to-all | bytes 8388608 | tf_op jit(solution)/shard_map/all_to_all | solution.py:14
  132.8 0.8 fusion.33
  135.1 1.9 copy.113
  137.0 10.1 %all-to-all-start.1 = ((bf16[16,32,1,16,128]{4,3,1,2,0:T(8,128)(2,1)}), bf16[16,32,1,16,128]{4,3,1,2,0:T(8,128)(2,1)}, u32[]{:S(2)}, u32[]{:S(2)}) async-start(bf16[16,32,1,16,128]{4,3,1,2,0:T(8,128)(2,1)} %bitcast.220), calls=%async_computation.1 | async-start | bytes 4194304 | tf_op jit(solution)/shard_map/all_to_all | solution.py:25
  148.8 0.8 fusion.14
  149.8 46.5 %all-to-all-done.1 = bf16[16,32,1,16,128]{4,3,1,2,0:T(8,128)(2,1)} async-done(((bf16[16,32,1,16,128]{4,3,1,2,0:T(8,128)(2,1)}), bf16[16,32,1,16,128]{4,3,1,2,0:T(8,128)(2,1)}, u32[]{:S(2)}, u32[]{:S(2)}) %all-to-all-start.1) | async-done | bytes 2097184 | tf_op jit(solution)/shard_map/all_to_all | solution.py:25
  196.2 2.6 reduce_sum.43
  198.8 5.3 %all-to-all-start.2 = ((bf16[32,16,128]{2,1,0:T(8,128)(2,1)}), bf16[32,16,128]{2,1,0:T(8,128)(2,1)S(1)}, u32[]{:S(2)}, u32[]{:S(2)}) async-start(bf16[32,16,128]{2,1,0:T(8,128)(2,1)} %reduce_sum.43), calls=%async_computation.2 | async-start | bytes 262144 | tf_op jit(solution)/shard_map/all_to_all | solution.py:154
  204.6 2.9 %fusion.5 = bf16[1,128,2048]{2,1,0:T(8,128)(2,1)} fusion(bf16[32,16,2048]{2,1,0:T(8,128)(2,1)} %bitcast.222, f32[32,16,128]{2,1,0:T(8,128)S(1)} %fusion.25, f32[32,16,128]{2,1,0:T(8,128)S(1)} %fusion.22), kind=kOutput, calls=%fused_computation.13 | convolution fusion | flops 269352960 | bytes 3145728 | tf_op jit(solution)/shard_map/secf,secd->efd/dot_general | solution.py:92
  207.6 6.0 %all-to-all-done.2 = bf16[32,16,128]{2,1,0:T(8,128)(2,1)S(1)} async-done(((bf16[32,16,128]{2,1,0:T(8,128)(2,1)}), bf16[32,16,128]{2,1,0:T(8,128)(2,1)S(1)}, u32[]{:S(2)}, u32[]{:S(2)}) %all-to-all-start.2) | async-done | bytes 131104 | tf_op jit(solution)/shard_map/all_to_all | solution.py:154
  213.6 1.0 gather_fusion
  214.7 1.4 constant_dynamic-update-slice_fusion.15
  225.4 1.3 copy.102
  226.7 1.0 copy.103
  227.7 6.4 %all-to-all-start.3 = ((bf16[128,16,128]{2,0,1:T(8,128)(2,1)}), bf16[128,16,128]{2,0,1:T(8,128)(2,1)S(1)}, u32[]{:S(2)}, u32[]{:S(2)}) async-start(bf16[128,16,128]{2,0,1:T(8,128)(2,1)} %copy.103), calls=%async_computation.3 | async-start | bytes 1048576 | tf_op jit(solution)/shard_map/all_to_all | solution.py:161
  234.2 1.6 fusion.4
  235.8 1.6 fusion.3
  237.3 14.0 %all-to-all-done.3 = bf16[128,16,128]{2,0,1:T(8,128)(2,1)S(1)} async-done(((bf16[128,16,128]{2,0,1:T(8,128)(2,1)}), bf16[128,16,128]{2,0,1:T(8,128)(2,1)S(1)}, u32[]{:S(2)}, u32[]{:S(2)}) %all-to-all-start.3) | async-done | bytes 524320 | tf_op jit(solution)/shard_map/all_to_all | solution.py:161
  251.7 0.8 fusion.54
  262.8 3.8 %all-to-all-start.5 = ((f32[32,2,32]{2,1,0:T(2,128)}), f32[32,2,32]{2,1,0:T(2,128)S(1)}, u32[]{:S(2)}, u32[]{:S(2)}) async-start(f32[32,2,32]{2,1,0:T(2,128)} %broadcast_in_dim.65), calls=%async_computation.5 | async-start | bytes 65536 | tf_op jit(solution)/shard_map/all_to_all | solution.py:31
  267.3 0.8 reshape.314
  268.2 7.1 %all-to-all-done.5 = f32[32,2,32]{2,1,0:T(2,128)S(1)} async-done(((f32[32,2,32]{2,1,0:T(2,128)}), f32[32,2,32]{2,1,0:T(2,128)S(1)}, u32[]{:S(2)}, u32[]{:S(2)}) %all-to-all-start.5) | async-done | bytes 8224 | tf_op jit(solution)/shard_map/all_to_all | solution.py:31
  275.3 3.8 %all-to-all-start.4 = ((bf16[32,2,1024]{2,1,0:T(2,128)(2,1)}), bf16[32,2,1024]{2,1,0:T(2,128)(2,1)S(1)}, u32[]{:S(2)}, u32[]{:S(2)}) async-start(bf16[32,2,1024]{2,1,0:T(2,128)(2,1)} %reshape.314), calls=%async_computation.4 | async-start | bytes 262144 | tf_op jit(solution)/shard_map/all_to_all | solution.py:25
  279.9 0.8 fusion.8
  280.7 8.3 %all-to-all-done.4 = bf16[32,2,1024]{2,1,0:T(2,128)(2,1)S(1)} async-done(((bf16[32,2,1024]{2,1,0:T(2,128)(2,1)}), bf16[32,2,1024]{2,1,0:T(2,128)(2,1)S(1)}, u32[]{:S(2)}, u32[]{:S(2)}) %all-to-all-start.4) | async-done | bytes 131104 | tf_op jit(solution)/shard_map/all_to_all | solution.py:25
  (207 shorter events, 31.8 us)
Async XLA Ops:
  0.6 131.1 %copy-start = (bf16[1,2048,128]{2,1,0:T(8,128)(2,1)S(1)}, bf16[1,2048,128]{2,1,0:T(8,128)(2,1)}, u32[]{:S(2)}) copy-start(bf16[1,2048,128]{2,1,0:T(8,128)(2,1)} %param.20) | copy-start | bytes 1572868
  0.6 5.9 %copy-start.3 = (bf16[128,2048]{1,0:T(8,128)(2,1)S(1)}, bf16[128,2048]{1,0:T(8,128)(2,1)}, u32[]{:S(2)}) copy-start(bf16[128,2048]{1,0:T(8,128)(2,1)} %param.17) | copy-start | bytes 1572868
  8.9 2.7 copy-start.12
  130.0 1.0 copy-start.2
  130.4 2.1 copy-start.1
  131.8 1.0 copy-start.16
  137.0 11.3 %copy-start.21 = (f32[32]{0:T(128)S(1)}, f32[32]{0:T(128)}, u32[]{:S(2)}) copy-start(f32[32]{0:T(128)} %param.30) | copy-start | bytes 388
  137.0 11.8 %copy-start.9 = (bf16[32,128]{1,0:T(8,128)(2,1)S(1)}, bf16[32,128]{1,0:T(8,128)(2,1)}, u32[]{:S(2)}) copy-start(bf16[32,128]{1,0:T(8,128)(2,1)} %param.25) | copy-start | bytes 24580
  137.0 11.8 %copy-start.17 = (bf16[1,32,32]{2,1,0:T(8,128)(2,1)S(1)}, bf16[1,32,32]{2,1,0:T(8,128)(2,1)}, u32[]{:S(2)}) copy-start(bf16[1,32,32]{2,1,0:T(8,128)(2,1)} %param.28) | copy-start | bytes 6148
  137.0 12.6 %copy-start.19 = (bf16[1,32,32]{2,1,0:T(8,128)(2,1)S(1)}, bf16[1,32,32]{2,1,0:T(8,128)(2,1)}, u32[]{:S(2)}) copy-start(bf16[1,32,32]{2,1,0:T(8,128)(2,1)} %param.29) | copy-start | bytes 6148
  137.0 59.2 %all-to-all-start.1 = ((bf16[16,32,1,16,128]{4,3,1,2,0:T(8,128)(2,1)}), bf16[16,32,1,16,128]{4,3,1,2,0:T(8,128)(2,1)}, u32[]{:S(2)}, u32[]{:S(2)}) async-start(bf16[16,32,1,16,128]{4,3,1,2,0:T(8,128)(2,1)} %bitcast.220), calls=%async_computation.1 | async-start | bytes 4194304 | tf_op jit(solution)/shard_map/all_to_all | solution.py:25
  198.8 14.8 %all-to-all-start.2 = ((bf16[32,16,128]{2,1,0:T(8,128)(2,1)}), bf16[32,16,128]{2,1,0:T(8,128)(2,1)S(1)}, u32[]{:S(2)}, u32[]{:S(2)}) async-start(bf16[32,16,128]{2,1,0:T(8,128)(2,1)} %reduce_sum.43), calls=%async_computation.2 | async-start | bytes 262144 | tf_op jit(solution)/shard_map/all_to_all | solution.py:154
  227.7 23.6 %all-to-all-start.3 = ((bf16[128,16,128]{2,0,1:T(8,128)(2,1)}), bf16[128,16,128]{2,0,1:T(8,128)(2,1)S(1)}, u32[]{:S(2)}, u32[]{:S(2)}) async-start(bf16[128,16,128]{2,0,1:T(8,128)(2,1)} %copy.103), calls=%async_computation.3 | async-start | bytes 1048576 | tf_op jit(solution)/shard_map/all_to_all | solution.py:161
  235.7 15.9 %copy-start.4 = (bf16[2048,32]{0,1:T(8,128)(2,1)S(1)}, bf16[2048,32]{0,1:T(8,128)(2,1)}, u32[]{:S(2)}) copy-start(bf16[2048,32]{0,1:T(8,128)(2,1)} %param.23) | copy-start | bytes 393220
  235.7 15.9 %copy-start.5 = (f32[32,128]{1,0:T(8,128)S(1)}, f32[32,128]{1,0:T(8,128)}, u32[]{:S(2)}) copy-start(f32[32,128]{1,0:T(8,128)} %param.31) | copy-start | bytes 49156
  235.7 15.9 %copy-start.6 = (f32[32,128]{1,0:T(8,128)S(1)}, f32[32,128]{1,0:T(8,128)}, u32[]{:S(2)}) copy-start(f32[32,128]{1,0:T(8,128)} %param.27) | copy-start | bytes 49156
  235.7 16.0 %copy-start.7 = (f32[32,128]{1,0:T(8,128)S(1)}, f32[32,128]{1,0:T(8,128)}, u32[]{:S(2)}) copy-start(f32[32,128]{1,0:T(8,128)} %fusion.14) | copy-start | bytes 49156
  235.7 16.0 %copy-start.8 = (bf16[32,128]{1,0:T(8,128)(2,1)S(1)}, bf16[32,128]{1,0:T(8,128)(2,1)}, u32[]{:S(2)}) copy-start(bf16[32,128]{1,0:T(8,128)(2,1)} %param.26) | copy-start | bytes 24580
  235.7 16.0 %copy-start.10 = (bf16[32,128]{1,0:T(8,128)(2,1)S(1)}, bf16[32,128]{1,0:T(8,128)(2,1)}, u32[]{:S(2)}) copy-start(bf16[32,128]{1,0:T(8,128)(2,1)} %param.25) | copy-start | bytes 24580
  235.8 16.0 %copy-start.13 = (f32[32]{0:T(128)S(1)}, f32[32]{0:T(128)}, u32[]{:S(2)}) copy-start(f32[32]{0:T(128)} %fusion.92) | copy-start | bytes 388
  235.8 16.0 %copy-start.14 = (pred[128]{0:T(512)(128)(4,1)S(1)}, pred[128]{0:T(512)(128)(4,1)}, u32[]{:S(2)}) copy-start(pred[128]{0:T(512)(128)(4,1)} %add_compare_fusion) | copy-start | bytes 388
  252.6 14.1 %copy-start.11 = (bf16[32,128]{1,0:T(8,128)(2,1)S(1)}, bf16[32,128]{1,0:T(8,128)(2,1)}, u32[]{:S(2)}) copy-start(bf16[32,128]{1,0:T(8,128)(2,1)} %param.24) | copy-start | bytes 24580
  258.2 20.9 %copy-start.15 = (pred[32]{0:T(512)(128)(4,1)S(1)}, pred[32]{0:T(512)(128)(4,1)}, u32[]{:S(2)}) copy-start(pred[32]{0:T(512)(128)(4,1)} %iota_compare_fusion.2) | copy-start | bytes 100
  259.6 20.1 %copy-start.18 = (bf16[1,32,32]{2,1,0:T(8,128)(2,1)S(1)}, bf16[1,32,32]{2,1,0:T(8,128)(2,1)}, u32[]{:S(2)}) copy-start(bf16[1,32,32]{2,1,0:T(8,128)(2,1)} %param.28) | copy-start | bytes 6148
  259.7 20.2 %copy-start.20 = (bf16[1,32,32]{2,1,0:T(8,128)(2,1)S(1)}, bf16[1,32,32]{2,1,0:T(8,128)(2,1)}, u32[]{:S(2)}) copy-start(bf16[1,32,32]{2,1,0:T(8,128)(2,1)} %param.29) | copy-start | bytes 6148
  262.8 12.5 %all-to-all-start.5 = ((f32[32,2,32]{2,1,0:T(2,128)}), f32[32,2,32]{2,1,0:T(2,128)S(1)}, u32[]{:S(2)}, u32[]{:S(2)}) async-start(f32[32,2,32]{2,1,0:T(2,128)} %broadcast_in_dim.65), calls=%async_computation.5 | async-start | bytes 65536 | tf_op jit(solution)/shard_map/all_to_all | solution.py:31
  275.3 13.7 %all-to-all-start.4 = ((bf16[32,2,1024]{2,1,0:T(2,128)(2,1)}), bf16[32,2,1024]{2,1,0:T(2,128)(2,1)S(1)}, u32[]{:S(2)}, u32[]{:S(2)}) async-start(bf16[32,2,1024]{2,1,0:T(2,128)(2,1)} %reshape.314), calls=%async_computation.4 | async-start | bytes 262144 | tf_op jit(solution)/shard_map/all_to_all | solution.py:25
